TPU v7x, 512 devices: a whole 4x4x16 slice. The times are simulated.
512 devices in a mesh: rep: 2 (over z_hi), fs: 32 (over z_lo, y), tp: 8 (over x, core).
Axes of the slice: x: 4, y: 4, z: 16 (z_hi: 2, z_lo: 8; z = z_hi * 8 + z_lo), core: 2. Of those that a mesh axis runs over, the one named last changes fastest.
Arguments:
- input_activation_entries: bfloat16 [24576, 2048], P(('rep', 'fs')), may hold values from -6 to 6
- premixing_rescale_factor: float32 [2048], replicated, may hold values from 0.1 to 1.9
- probe_weight_table: float32 [2048, 1024], P('fs', 'tp'), may hold values from -0.125 to 0.125
- probe_factor_list: float32 [1024], P('tp'), may hold values from 0.5 to 2
- lookup_weight_table: float32 [2048, 1024], P('fs', 'tp'), may hold values from -0.125 to 0.125
- lookup_factor_list: float32 [1024], P('tp'), may hold values from 0.5 to 2
- forget_weight_table: float32 [2048, 1024], P('fs', 'tp'), may hold values from -0.125 to 0.125
- forget_factor_list: float32 [1024], P('tp'), may hold values from 1 to 8
- forget_shift_term: float32 [1024], P('tp'), may hold values from -3 to 7
- extra_forget_logs: float32 [24576, 8], P(('rep', 'fs'), 'tp'), may hold values from -0.7 to 0
- content_weight_table: float32 [2048, 2048], P('fs', 'tp'), may hold values from -0.125 to 0.125
- content_factor_list: float32 [2048], P('tp'), may hold values from 0.5 to 2
- filter_weight_table: float32 [2048, 2048], P('fs', 'tp'), may hold values from -0.125 to 0.125
- filter_factor_list: float32 [2048], P('tp'), may hold values from 0.5 to 2
- per_group_rescale_factor: float32 [2048], P('tp'), may hold values from 0.1 to 1.9
- emission_weight_table: float32 [2048, 2048], P('tp', 'fs'), may hold values from -0.125 to 0.125
- emission_factor_list: float32 [2048], P('fs'), may hold values from 0.5 to 2
- perceptron_prenorm_factor: float32 [2048], replicated, may hold values from 0.1 to 1.9
- raising_weight_table: float32 [2048, 8192], P('fs', 'tp'), may hold values from -0.125 to 0.125
- raising_factor_list: float32 [8192], P('tp'), may hold values from 0.5 to 2
- lowering_weight_table: float32 [8192, 2048], P('tp', 'fs'), may hold values from -0.0625 to 0.0625
- lowering_factor_list: float32 [2048], P('fs'), may hold values from 0.5 to 2
Outputs:
- layer_out: bfloat16 [24576, 2048], P(('rep', 'fs'))
All inputs are finite; a program needn't handle non-finite values.
Results may differ from a plain program's by a relative error of at most 0.02.
Values may be sent and summed in bfloat16 or wider, within the bound.
No kernel may reach another device: no remote copies, remote signals or barrier semaphores. Data moves between devices by JAX's collectives and lax.ppermute only.
A program may use at most 64 MiB of HBM per device.

v0:
```python
import jax
import jax.numpy as jnp
from jax import lax
from jax.sharding import PartitionSpec as P

LOOKUP_FEATURES = 128
BLOCK = 64
epsilon = 1e-06
filter_rescaled_entries = 16.0
highest = lax.Precision.HIGHEST


def rows_first(arrays, axis, dims):
    turned = [jnp.moveaxis(a, dim, 0) for a, dim in zip(arrays, dims)]
    widths = [t[0].size for t in turned]
    both = jnp.concatenate([t.reshape(-1, w) for t, w in zip(turned, widths)], axis=1)
    filled = lax.all_gather(both, axis, axis=0, tiled=True)
    pieces = jnp.split(filled, [sum(widths[:k]) for k in range(1, len(widths))], axis=1)
    return tuple(
        (
            jnp.moveaxis(b.reshape(-1, *t.shape[1:]), 0, dim)
            for b, t, dim in zip(pieces, turned, dims)
        )
    )


def cut_along(value, dim, devices):
    before, after = (value.shape[:dim], value.shape[dim + 1 :])
    return jnp.moveaxis(value.reshape(*before, devices, -1, *after), dim, 0)


def sent_and_summed(value, axis, dim):
    pieces = cut_along(value, dim, lax.axis_size(axis))
    arrived = lax.all_to_all(pieces, axis, split_axis=0, concat_axis=0, tiled=True)
    return arrived.astype(jnp.float32).sum(axis=0)


def laid_out(pieces, dim):
    dims = list(pieces.shape[1:])
    dims[dim] *= pieces.shape[0]
    return jnp.moveaxis(pieces, 0, dim).reshape(dims)


def from_everyone(value, axis):
    devices = lax.axis_size(axis)
    return lax.all_to_all(
        jnp.broadcast_to(value[None], (devices, *value.shape)), axis, 0, 0, tiled=True
    )


def gathered_copies(value, axis, dim):
    return laid_out(from_everyone(value, axis), dim)


def rms_rows(matrix, gain):
    matrix = matrix.astype(jnp.float32)
    return matrix * lax.rsqrt(jnp.mean(matrix * matrix, axis=-1, keepdims=True) + epsilon) * gain


def recur_head(queries, keys_in, vals, forget_log_rate):
    length = queries.shape[0]
    blocks = length // BLOCK

    def to_blocks(tensor):
        return tensor.astype(jnp.float32).reshape(blocks, BLOCK, tensor.shape[-1])

    causal = jnp.tril(jnp.ones((BLOCK, BLOCK), dtype=bool))[:, :, None]

    def advance(memory, inputs):
        query_block, key_block, value_block, decay_block = inputs
        cumulative = jnp.cumsum(decay_block, axis=0)
        spread = cumulative[:, None, :] - cumulative[None, :, :]
        weights = jnp.exp(jnp.where(causal, spread, -jnp.inf))
        scores = jnp.einsum("tc,sc,tsc->ts", query_block, key_block, weights, precision=highest)
        within = jnp.dot(scores, value_block, precision=highest)
        carried = jnp.dot(query_block * jnp.exp(cumulative), memory, precision=highest)
        closing = cumulative[-1]
        scaled_keys = key_block * jnp.exp(closing[None, :] - cumulative)
        memory = jnp.exp(closing)[:, None] * memory + jnp.dot(
            scaled_keys.T, value_block, precision=highest
        )
        return (memory, within + carried)

    initial = jnp.zeros((queries.shape[-1], vals.shape[-1]), jnp.float32)
    _, outputs = lax.scan(
        advance,
        initial,
        (to_blocks(queries), to_blocks(keys_in), to_blocks(vals), to_blocks(forget_log_rate)),
    )
    return outputs.reshape(length, vals.shape[-1])


def per_group_mixing_values(
    probe_mapped_entries,
    lookup_mapped_entries,
    forget_mapped_entries,
    content_mapped_entries,
    filter_mapped_entries,
    forget_shift_term,
    extra_forget_logs,
    per_group_rescale_factor,
):
    group_count_total = extra_forget_logs.shape[-1]
    queries = (jax.nn.silu(probe_mapped_entries) * LOOKUP_FEATURES ** (-0.5)).astype(jnp.bfloat16)
    keyed = jax.nn.silu(lookup_mapped_entries).astype(jnp.bfloat16)
    valued = jax.nn.silu(content_mapped_entries).astype(jnp.bfloat16)
    forget_log_rate = jax.nn.log_sigmoid(
        forget_mapped_entries + forget_shift_term
    ) / filter_rescaled_entries + jnp.repeat(extra_forget_logs, LOOKUP_FEATURES, axis=1)

    def by_head(tensor):
        return tensor.reshape(tensor.shape[0], group_count_total, -1).transpose(1, 0, 2)

    outputs = jax.vmap(recur_head)(
        by_head(queries), by_head(keyed), by_head(valued), by_head(forget_log_rate)
    )
    outputs = outputs * lax.rsqrt(jnp.mean(outputs * outputs, axis=-1, keepdims=True) + epsilon)
    merged = outputs.transpose(1, 0, 2).reshape(outputs.shape[1], -1)
    return (merged * per_group_rescale_factor * jax.nn.silu(filter_mapped_entries)).astype(
        jnp.bfloat16
    )


def body(
    input_activation_entries,
    premixing_rescale_factor,
    probe_weight_table,
    probe_factor_list,
    lookup_weight_table,
    lookup_factor_list,
    forget_weight_table,
    forget_factor_list,
    forget_shift_term,
    extra_forget_logs,
    content_weight_table,
    content_factor_list,
    filter_weight_table,
    filter_factor_list,
    per_group_rescale_factor,
    emission_weight_table,
    emission_factor_list,
    perceptron_prenorm_factor,
    raising_weight_table,
    raising_factor_list,
    lowering_weight_table,
    lowering_factor_list,
):
    whole_out_scale, whole_down_scale = rows_first(
        (emission_factor_list, lowering_factor_list), "fs", (0, 0)
    )
    normed = rms_rows(input_activation_entries, premixing_rescale_factor).astype(jnp.bfloat16)
    query_bf = probe_weight_table.astype(jnp.bfloat16)
    key_bf = lookup_weight_table.astype(jnp.bfloat16)
    decay_bf = forget_weight_table.astype(jnp.bfloat16)
    value_bf = content_weight_table.astype(jnp.bfloat16)
    gate_bf = filter_weight_table.astype(jnp.bfloat16)
    out_bf = emission_weight_table.astype(jnp.bfloat16)
    up_bf = raising_weight_table.astype(jnp.bfloat16)
    down_bf = lowering_weight_table.astype(jnp.bfloat16)
    share_rows = input_activation_entries.shape[0] // lax.axis_size("tp")
    share_start = lax.axis_index("tp") * share_rows
    collected = rows_first(
        (query_bf, key_bf, decay_bf, value_bf, gate_bf, up_bf, out_bf, down_bf),
        "fs",
        (0, 0, 0, 0, 0, 0, 1, 1),
    )
    projected = tuple(
        (jnp.dot(normed, matrix, preferred_element_type=jnp.float32) for matrix in collected[:5])
    )
    mixing_product = per_group_mixing_values(
        projected[0] * probe_factor_list,
        projected[1] * lookup_factor_list,
        projected[2] * forget_factor_list,
        projected[3] * content_factor_list,
        projected[4] * filter_factor_list,
        forget_shift_term,
        extra_forget_logs,
        per_group_rescale_factor,
    )
    mix_part = (
        jnp.dot(mixing_product, collected[6], preferred_element_type=jnp.float32) * whole_out_scale
    )
    mix_rounded = lax.optimization_barrier(mix_part.astype(jnp.bfloat16)).astype(jnp.float32)
    mix_share = sent_and_summed(mix_rounded.astype(jnp.bfloat16), "tp", 0)
    token_share = lax.dynamic_slice_in_dim(input_activation_entries, share_start, share_rows, 0)
    residual = (token_share.astype(jnp.float32) + mix_share).astype(jnp.bfloat16)
    normed_share = rms_rows(residual, perceptron_prenorm_factor).astype(jnp.bfloat16)
    normed_mlp = gathered_copies(normed_share, "tp", 0)
    lifted = jnp.dot(normed_mlp, collected[5], preferred_element_type=jnp.float32)
    hidden = jnp.square(jax.nn.relu(lifted * raising_factor_list)).astype(jnp.bfloat16)
    mlp_part = jnp.dot(hidden, collected[7], preferred_element_type=jnp.float32) * whole_down_scale
    mlp_rounded = lax.optimization_barrier(mlp_part.astype(jnp.bfloat16)).astype(jnp.float32)
    mlp_share = sent_and_summed(mlp_rounded.astype(jnp.bfloat16), "tp", 0)
    out_share = (residual.astype(jnp.float32) + mlp_share).astype(jnp.bfloat16)
    return gathered_copies(out_share, "tp", 0)


def solution(mesh):
    return jax.shard_map(
        body,
        mesh=mesh,
        in_specs=(
            P(("rep", "fs"), None),
            P(),
            P("fs", "tp"),
            P("tp"),
            P("fs", "tp"),
            P("tp"),
            P("fs", "tp"),
            P("tp"),
            P("tp"),
            P(("rep", "fs"), "tp"),
            P("fs", "tp"),
            P("tp"),
            P("fs", "tp"),
            P("tp"),
            P("tp"),
            P("tp", "fs"),
            P("fs"),
            P(),
            P("fs", "tp"),
            P("tp"),
            P("tp", "fs"),
            P("fs"),
        ),
        out_specs=P(("rep", "fs"), None),
        check_vma=False,
    )
```

profile of v0, /device:TPU:1, one launch (start us, length us, event | category | flops | bytes accessed | tf_op | source)
XLA Modules:
  0.0 413.1 jit_solution(14367460227402730513)
XLA Ops:
  10.6 1.0 convert_dynamic-update-slice_fusion
  12.5 1.0 bitcast_dynamic-update-slice_fusion
  15.0 114.9 %all-gather = f32[32,64,2]{1,2,0:T(2,128)S(1)} all-gather(f32[1,64,2]{1,2,0:T(2,128)S(1)} %maximum_bitcast_fusion), channel_id=1, replica_groups=mesh['rep'=2,'fs'=32,'tp'=8] {'fs'}, dimensions={0}, use_global_device_ids=true | all-gather | bytes 16896 | tf_op jit(solution)/shard_map/all_gather | solution.py:17
  131.5 115.5 %all-gather.3.cloned.1.call-done = bf16[2048,3200]{1,0:T(8,128)(2,1)} async-done(((bf16[64,3200]{1,0:T(8,128)(2,1)}), bf16[2048,3200]{1,0:T(8,128)(2,1)}) %all-gather.3.cloned.1.call-update) | async-done | bytes 13107216 | tf_op jit(solution)/shard_map/all_gather | solution.py:17
  247.0 1.8 multiply_convert_fusion.3
  248.9 2.2 multiply_convert_fusion.5
  251.2 1.6 multiply_convert_fusion.4
  252.9 1.7 fusion.67
  254.7 20.3 %while.13 = (s32[]{:T(128)}, f32[1,128,256]{2,1,0:T(8,128)S(1)}, f32[6,1,64,256]{3,2,1,0:T(8,128)S(1)}, f32[6,1,64,128]{3,2,1,0:T(8,128)S(1)}, f32[6,1,64,128]{3...) while((s32[]{:T(128)}, f32[1,128,256]{2,1,0:T(8,128)S(1)}, ...), condition=%wide.region_3.4_spmd.clone, body=%wide.region_1.3_spmd.clone.sunk | while | flops 66224128 | bytes 5469312 | solution.py:85
  255.5 1.7 fusion.105
  258.8 1.7 fusion.105
  262.2 1.7 fusion.105
  265.6 1.7 fusion.105
  269.0 1.7 fusion.105
  272.4 1.7 fusion.105
  275.2 2.3 fusion.60
  277.5 3.0 multiply_convert_fusion.1
  280.5 23.9 %all-to-all-start = ((bf16[8,48,2048]{2,1,0:T(8,128)(2,1)}), bf16[8,48,2048]{2,1,0:T(8,128)(2,1)S(1)}, u32[]{:S(2)}, u32[]{:S(2)}) async-start(bf16[8,48,2048]{2,1,0:T(8,128)(2,1)} %bitcast.150), calls=%async_computation | async-start | bytes 3145728 | tf_op jit(solution)/shard_map/all_to_all | solution.py:34
  304.4 20.6 %all-to-all-done = bf16[8,48,2048]{2,1,0:T(8,128)(2,1)S(1)} async-done(((bf16[8,48,2048]{2,1,0:T(8,128)(2,1)}), bf16[8,48,2048]{2,1,0:T(8,128)(2,1)S(1)}, u32[]{:S(2)}, u32[]{:S(2)}) %all-to-all-start) | async-done | bytes 1572896 | tf_op jit(solution)/shard_map/all_to_all | solution.py:34
  325.8 24.0 %all_to_all.20 = bf16[8,48,2048]{2,1,0:T(8,128)(2,1)S(1)} all-to-all(bf16[8,48,2048]{2,1,0:T(8,128)(2,1)S(1)} %broadcast_in_dim.33), channel_id=1, replica_groups=mesh['rep'=2,'fs'=32,'tp'=8] {'tp'}, dimensions={0} | all-to-all | bytes 3145728 | tf_op jit(solution)/shard_map/all_to_all | solution.py:46
  349.7 6.9 %multiply_convert_fusion = bf16[384,2048]{1,0:T(8,128)(2,1)S(1)} fusion(bf16[2048,3200]{1,0:T(8,128)(2,1)} %all-gather.3.cloned.1.call-done, f32[2048]{0:T(1024)S(1)} %bitcast.157, bf16[384,2048]{1,0:T(8,128)(2,1)S(1)} %bitcast.151, f32[1024]{0:T(1024)S(1)} %copy-done.7), kind=kOutput, calls=%fused_computation.49 | convolution fusion | flops 3224371200 | bytes 11546624 | tf_op jit(solution)/shard_map/dot_general | solution.py:191
  356.6 24.0 %all_to_all.21 = bf16[8,48,2048]{2,1,0:T(8,128)(2,1)S(1)} all-to-all(bf16[8,48,2048]{2,1,0:T(8,128)(2,1)S(1)} %bitcast.152), channel_id=1, replica_groups=mesh['rep'=2,'fs'=32,'tp'=8] {'tp'}, dimensions={0} | all-to-all | bytes 3145728 | tf_op jit(solution)/shard_map/all_to_all | solution.py:34
  381.1 24.0 %all_to_all.22 = bf16[8,48,2048]{2,1,0:T(8,128)(2,1)S(1)} all-to-all(bf16[8,48,2048]{2,1,0:T(8,128)(2,1)S(1)} %broadcast_in_dim.34), channel_id=1, replica_groups=mesh['rep'=2,'fs'=32,'tp'=8] {'tp'}, dimensions={0} | all-to-all | bytes 3145728 | tf_op jit(solution)/shard_map/all_to_all | solution.py:46
  405.1 1.1 copy.74
  (122 shorter events, 19.1 us)
Async XLA Ops:
  6.5 124.1 %copy-start = (bf16[384,2048]{1,0:T(8,128)(2,1)S(1)}, bf16[384,2048]{1,0:T(8,128)(2,1)}, u32[]{:S(2)}) copy-start(bf16[384,2048]{1,0:T(8,128)(2,1)} %param.24) | copy-start | bytes 4718596
  6.5 124.5 %copy-start.5 = (f32[2048]{0:T(1024)S(1)}, f32[2048]{0:T(1024)}, u32[]{:S(2)}) copy-start(f32[2048]{0:T(1024)} %param.25) | copy-start | bytes 24580
  6.5 240.5 %all-gather.3.cloned.1.call-start = ((), (), s32[]{:S(2)}) async-start(), calls=%async_computation.4 | async-start | bytes 13516800 | tf_op jit(solution)/shard_map/all_gather | solution.py:17
  13.4 0.8 copy-start.3
  130.6 116.4 %copy-start.8 = (f32[256]{0:T(256)S(1)}, f32[256]{0:T(256)}, u32[]{:S(2)}) copy-start(f32[256]{0:T(256)} %param.35) | copy-start | bytes 3076
  131.5 117.4 %copy-start.1 = (bf16[384,2048]{1,0:T(8,128)(2,1)}, bf16[384,2048]{1,0:T(8,128)(2,1)S(1)}, u32[]{:S(2)}) copy-start(bf16[384,2048]{1,0:T(8,128)(2,1)S(1)} %fusion.37) | copy-start | bytes 4718596
  131.5 117.4 %copy-start.11 = (f32[128]{0:T(128)S(1)}, f32[128]{0:T(128)}, u32[]{:S(2)}) copy-start(f32[128]{0:T(128)} %param.29) | copy-start | bytes 1540
  248.9 2.3 copy-start.12
  248.9 2.3 copy-start.2
  251.2 1.7 copy-start.13
  251.2 1.7 copy-start.14
  252.9 1.8 copy-start.4
  254.7 20.6 %copy-start.9 = (f32[256]{0:T(256)S(1)}, f32[256]{0:T(256)}, u32[]{:S(2)}) copy-start(f32[256]{0:T(256)} %param.37) | copy-start | bytes 3076
  254.7 20.6 %copy-start.10 = (f32[256]{0:T(256)S(1)}, f32[256]{0:T(256)}, u32[]{:S(2)}) copy-start(f32[256]{0:T(256)} %param.38) | copy-start | bytes 3076
  280.5 44.5 %all-to-all-start = ((bf16[8,48,2048]{2,1,0:T(8,128)(2,1)}), bf16[8,48,2048]{2,1,0:T(8,128)(2,1)S(1)}, u32[]{:S(2)}, u32[]{:S(2)}) async-start(bf16[8,48,2048]{2,1,0:T(8,128)(2,1)} %bitcast.150), calls=%async_computation | async-start | bytes 3145728 | tf_op jit(solution)/shard_map/all_to_all | solution.py:34
  304.4 21.0 %copy-start.6 = (f32[2048]{0:T(1024)S(1)}, f32[2048]{0:T(1024)}, u32[]{:S(2)}) copy-start(f32[2048]{0:T(1024)} %param.41) | copy-start | bytes 24580
  325.6 24.2 %copy-start.7 = (f32[1024]{0:T(1024)S(1)}, f32[1024]{0:T(1024)}, u32[]{:S(2)}) copy-start(f32[1024]{0:T(1024)} %param.43) | copy-start | bytes 12292
Sparse Core Ops, SparseCore 0:
  14.4 232.6 all-gather.2
where the time goes:
time: 414 us; the launch traced here: 413 us
  blocking collectives  187 us (45%)
  waiting for transfers between devices  136 us (33%)
  other arithmetic  24.6 us (6%)
  matrix products  24.6 us (6%)
  starting transfers between devices  23.9 us (6%)
  between operations  13.7 us (3%)
    all_gather x1, waiting for transfers between devices, rows_first(): filled = lax.all_gather(both, axis, axis=0, tiled=True)  116 us
    all_gather x1, blocking collectives, rows_first(): filled = lax.all_gather(both, axis, axis=0, tiled=True)  115 us
    all_to_all x2, blocking collectives, from_everyone(): lax.all_to_all(jnp.broadcast_to(value[None], (devices, *value.shape)), ax...  48 us
    all_to_all x1, blocking collectives, sent_and_summed(): lax.all_to_all(pieces, axis, split_axis=0, concat_axis=0, tiled=True)  24 us
    all_to_all x1, starting transfers between devices, sent_and_summed(): lax.all_to_all(pieces, axis, split_axis=0, concat_axis=0, tiled=True)  23.9 us
    all_to_all x1, waiting for transfers between devices, sent_and_summed(): lax.all_to_all(pieces, axis, split_axis=0, concat_axis=0, tiled=True)  20.6 us
    dot_general x6, other arithmetic, advance(): jnp.einsum('tc,sc,tsc->ts', query_block, key_block, weights, precision=hi...  10.2 us
    dot_general x5, matrix products, body(): jnp.dot(normed, matrix, preferred_element_type=jnp.float32)  9.67 us
  transfers between devices with their start and end apart: 2, of which 2 were waited for; matrix products, arithmetic and copies ran while one was open for 1% of the time, Pallas kernels for 0%

commit v1 on v0

--- a/solution.py
+++ b/solution.py
@@ -14,7 +14,10 @@
     turned = [jnp.moveaxis(a, dim, 0) for a, dim in zip(arrays, dims)]
     widths = [t[0].size for t in turned]
     both = jnp.concatenate([t.reshape(-1, w) for t, w in zip(turned, widths)], axis=1)
-    filled = lax.all_gather(both, axis, axis=0, tiled=True)
+    size = lax.axis_size(axis)
+    parts = jnp.stack([both for _ in range(size)])
+    parts = lax.all_to_all(parts, axis, split_axis=0, concat_axis=0)
+    filled = jnp.concatenate(parts, axis=0)
     pieces = jnp.split(filled, [sum(widths[:k]) for k in range(1, len(widths))], axis=1)
     return tuple(
         (

time: 414 us -> 764 us (1.85)
  waiting for transfers between devices: 136 us -> 601 us
  blocking collectives: 187 us -> 72 us
  between operations: 13.7 us -> 0.38 us
    all_to_all x0 -> x2, waiting for transfers between devices: none -> 581 us  [rows_first(): parts = lax.all_to_all(parts, axis, split_axis=0, concat_axis=0)]
    all_gather x1 -> x0, waiting for transfers between devices: 116 us -> none  [rows_first(): filled = lax.all_gather(both, axis, axis=0, tiled=True)]
    all_gather x1 -> x0, blocking collectives: 115 us -> none  [rows_first(): filled = lax.all_gather(both, axis, axis=0, tiled=True)]
    all_to_all x0 -> x2, starting transfers between devices: none -> 23.7 us  [rows_first(): parts = lax.all_to_all(parts, axis, split_axis=0, concat_axis=0)]
    all_to_all x1, starting transfers between devices: 23.9 us -> 6.67 us  [sent_and_summed(): lax.all_to_all(pieces, axis, split_axis=0, concat_axis=0, tiled=True)]
  transfers between devices with their start and end apart: 2 -> 3, of which waited for: 2 -> 3; matrix products, arithmetic and copies ran while one was open for 1% -> 1% of each run, Pallas kernels for 0% -> 0%
where the time goes in v1:
time: 764 us; the launch traced here: 763 us
  waiting for transfers between devices  601 us (79%)
  blocking collectives  72 us (9%)
  starting transfers between devices  30.4 us (4%)
  matrix products  24.6 us (3%)
  other arithmetic  24.4 us (3%)
  local copies, waits for them, and re-layouts  9.74 us (1%)
    all_to_all x2, waiting for transfers between devices, rows_first(): parts = lax.all_to_all(parts, axis, split_axis=0, concat_axis=0)  581 us
    all_to_all x2, blocking collectives, from_everyone(): lax.all_to_all(jnp.broadcast_to(value[None], (devices, *value.shape)), ax...  48 us
    all_to_all x1, blocking collectives, sent_and_summed(): lax.all_to_all(pieces, axis, split_axis=0, concat_axis=0, tiled=True)  24 us
    all_to_all x2, starting transfers between devices, rows_first(): parts = lax.all_to_all(parts, axis, split_axis=0, concat_axis=0)  23.7 us
    all_to_all x1, waiting for transfers between devices, sent_and_summed(): lax.all_to_all(pieces, axis, split_axis=0, concat_axis=0, tiled=True)  20.6 us
  transfers between devices with their start and end apart: 3, of which 3 were waited for; matrix products, arithmetic and copies ran while one was open for 1% of the time, Pallas kernels for 0%

profile of v1, /device:TPU:1, one launch (start us, length us, event | category | flops | bytes accessed | tf_op | source)
XLA Modules:
  0.0 763.3 jit_solution(6993578968765375652)
XLA Ops:
  1.4 16.1 %all-to-all-start.1 = ((f32[32,1,128]{2,1,0:T(1,128)}), f32[32,1,128]{2,1,0:T(1,128)S(1)}, u32[]{:S(2)}, u32[]{:S(2)}) async-start(f32[32,1,128]{2,1,0:T(1,128)} %reshape.293), calls=%async_computation.1 | async-start | bytes 32768 | tf_op jit(solution)/shard_map/all_to_all | solution.py:19
  24.3 4.6 all-to-all-done.1
  28.9 6.4 stack.4
  35.3 7.6 %all-to-all-start = ((bf16[32,64,3200]{2,1,0:T(8,128)(2,1)}), bf16[32,64,3200]{2,1,0:T(8,128)(2,1)}, u32[]{:S(2)}, u32[]{:S(2)}) async-start(bf16[32,64,3200]{2,1,0:T(8,128)(2,1)} %stack.4), calls=%async_computation | async-start | bytes 26214400 | tf_op jit(solution)/shard_map/all_to_all | solution.py:19
  45.2 576.1 %all-to-all-done = bf16[32,64,3200]{2,1,0:T(8,128)(2,1)} async-done(((bf16[32,64,3200]{2,1,0:T(8,128)(2,1)}), bf16[32,64,3200]{2,1,0:T(8,128)(2,1)}, u32[]{:S(2)}, u32[]{:S(2)}) %all-to-all-start) | async-done | bytes 13107232 | tf_op jit(solution)/shard_map/all_to_all | solution.py:19
  621.3 1.8 multiply_convert_fusion.3
  623.3 2.2 multiply_convert_fusion.5
  625.5 1.6 multiply_convert_fusion.4
  627.2 1.7 fusion.67
  629.0 20.3 %while.13 = (s32[]{:T(128)}, f32[1,128,256]{2,1,0:T(8,128)S(1)}, f32[6,1,64,256]{3,2,1,0:T(8,128)S(1)}, f32[6,1,64,128]{3,2,1,0:T(8,128)S(1)}, f32[6,1,64,128]{3...) while((s32[]{:T(128)}, f32[1,128,256]{2,1,0:T(8,128)S(1)}, ...), condition=%wide.region_3.4_spmd.clone, body=%wide.region_1.3_spmd.clone.sunk | while | flops 66224128 | bytes 5469312 | solution.py:88
  629.8 1.7 fusion.105
  633.2 1.7 fusion.105
  636.5 1.7 fusion.105
  639.9 1.7 fusion.105
  643.3 1.7 fusion.105
  646.7 1.7 fusion.105
  649.5 2.3 fusion.60
  651.8 3.0 multiply_convert_fusion.1
  654.8 6.7 all-to-all-start.2
  661.5 20.6 %all-to-all-done.2 = bf16[8,48,2048]{2,1,0:T(8,128)(2,1)S(1)} async-done(((bf16[8,48,2048]{2,1,0:T(8,128)(2,1)}), bf16[8,48,2048]{2,1,0:T(8,128)(2,1)S(1)}, u32[]{:S(2)}, u32[]{:S(2)}) %all-to-all-start.2) | async-done | bytes 1572896 | tf_op jit(solution)/shard_map/all_to_all | solution.py:37
  682.8 24.0 %all_to_all.30 = bf16[8,48,2048]{2,1,0:T(8,128)(2,1)S(1)} all-to-all(bf16[8,48,2048]{2,1,0:T(8,128)(2,1)S(1)} %broadcast_in_dim.33), channel_id=1, replica_groups=mesh['rep'=2,'fs'=32,'tp'=8] {'tp'}, dimensions={0} | all-to-all | bytes 3145728 | tf_op jit(solution)/shard_map/all_to_all | solution.py:49
  706.8 6.9 multiply_convert_fusion
  713.7 24.0 %all_to_all.31 = bf16[8,48,2048]{2,1,0:T(8,128)(2,1)S(1)} all-to-all(bf16[8,48,2048]{2,1,0:T(8,128)(2,1)S(1)} %bitcast.154), channel_id=1, replica_groups=mesh['rep'=2,'fs'=32,'tp'=8] {'tp'}, dimensions={0} | all-to-all | bytes 3145728 | tf_op jit(solution)/shard_map/all_to_all | solution.py:37
  738.2 24.0 %all_to_all.32 = bf16[8,48,2048]{2,1,0:T(8,128)(2,1)S(1)} all-to-all(bf16[8,48,2048]{2,1,0:T(8,128)(2,1)S(1)} %broadcast_in_dim.34), channel_id=1, replica_groups=mesh['rep'=2,'fs'=32,'tp'=8] {'tp'}, dimensions={0} | all-to-all | bytes 3145728 | tf_op jit(solution)/shard_map/all_to_all | solution.py:49
  (128 shorter events, 22.6 us)
Async XLA Ops:
  1.4 27.5 %all-to-all-start.1 = ((f32[32,1,128]{2,1,0:T(1,128)}), f32[32,1,128]{2,1,0:T(1,128)S(1)}, u32[]{:S(2)}, u32[]{:S(2)}) async-start(f32[32,1,128]{2,1,0:T(1,128)} %reshape.293), calls=%async_computation.1 | async-start | bytes 32768 | tf_op jit(solution)/shard_map/all_to_all | solution.py:19
  35.3 7.7 %copy-start.6 = (f32[384,1]{0,1:T(1,128)S(1)}, f32[384,1]{0,1:T(1,128)}, u32[]{:S(2)}) copy-start(f32[384,1]{0,1:T(1,128)} %param.33) | copy-start | bytes 4612
  35.3 7.7 %copy-start = (bf16[384,2048]{1,0:T(8,128)(2,1)S(1)}, bf16[384,2048]{1,0:T(8,128)(2,1)}, u32[]{:S(2)}) copy-start(bf16[384,2048]{1,0:T(8,128)(2,1)} %param.24) | copy-start | bytes 4718596
  35.3 8.1 %copy-start.4 = (f32[2048]{0:T(1024)S(1)}, f32[2048]{0:T(1024)}, u32[]{:S(2)}) copy-start(f32[2048]{0:T(1024)} %param.25) | copy-start | bytes 24580
  35.3 586.0 %all-to-all-start = ((bf16[32,64,3200]{2,1,0:T(8,128)(2,1)}), bf16[32,64,3200]{2,1,0:T(8,128)(2,1)}, u32[]{:S(2)}, u32[]{:S(2)}) async-start(bf16[32,64,3200]{2,1,0:T(8,128)(2,1)} %stack.4), calls=%async_computation | async-start | bytes 26214400 | tf_op jit(solution)/shard_map/all_to_all | solution.py:19
  43.0 578.3 %copy-start.8 = (f32[256]{0:T(256)S(1)}, f32[256]{0:T(256)}, u32[]{:S(2)}) copy-start(f32[256]{0:T(256)} %param.35) | copy-start | bytes 3076
  43.9 579.3 %copy-start.1 = (bf16[384,2048]{1,0:T(8,128)(2,1)}, bf16[384,2048]{1,0:T(8,128)(2,1)S(1)}, u32[]{:S(2)}) copy-start(bf16[384,2048]{1,0:T(8,128)(2,1)S(1)} %fusion.37) | copy-start | bytes 4718596
  621.3 1.9 copy-start.11
  623.2 2.3 copy-start.12
  623.2 2.3 copy-start.2
  625.5 1.7 copy-start.13
  625.5 1.7 copy-start.14
  627.2 1.8 copy-start.3
  629.0 20.6 %copy-start.9 = (f32[256]{0:T(256)S(1)}, f32[256]{0:T(256)}, u32[]{:S(2)}) copy-start(f32[256]{0:T(256)} %param.37) | copy-start | bytes 3076
  629.0 20.6 %copy-start.10 = (f32[256]{0:T(256)S(1)}, f32[256]{0:T(256)}, u32[]{:S(2)}) copy-start(f32[256]{0:T(256)} %param.38) | copy-start | bytes 3076
  654.8 27.3 %all-to-all-start.2 = ((bf16[8,48,2048]{2,1,0:T(8,128)(2,1)}), bf16[8,48,2048]{2,1,0:T(8,128)(2,1)S(1)}, u32[]{:S(2)}, u32[]{:S(2)}) async-start(bf16[8,48,2048]{2,1,0:T(8,128)(2,1)} %bitcast.152), calls=%async_computation.2 | async-start | bytes 3145728 | tf_op jit(solution)/shard_map/all_to_all | solution.py:37
  661.5 21.0 %copy-start.5 = (f32[2048]{0:T(1024)S(1)}, f32[2048]{0:T(1024)}, u32[]{:S(2)}) copy-start(f32[2048]{0:T(1024)} %param.41) | copy-start | bytes 24580
  682.6 24.2 %copy-start.7 = (f32[1024]{0:T(1024)S(1)}, f32[1024]{0:T(1024)}, u32[]{:S(2)}) copy-start(f32[1024]{0:T(1024)} %param.43) | copy-start | bytes 12292
